TPU v7x, 32 devices: a whole 2x2x4 slice. The times are simulated.
32 devices in a mesh: tp: 8 (over z, y), dp: 4 (over x, core).
Axes of the slice: x: 2, y: 2, z: 4, core: 2. Of those that a mesh axis runs over, the one named last changes fastest.
Arguments:
- stream: bfloat16 [32, 4096], P('dp', 'tp'), may hold values from -6 to 6
- query_weight: bfloat16 [2, 4096, 3072], P(None, 'dp', 'tp'), may hold values from -0.09375 to 0.09375
- key_weight: bfloat16 [2, 4096, 3072], P(None, 'dp', 'tp'), may hold values from -0.09375 to 0.09375
- value_weight: bfloat16 [2, 4096, 3072], P(None, 'dp', 'tp'), may hold values from -0.09375 to 0.09375
- outgate_weight: bfloat16 [2, 4096, 3072], P(None, 'dp', 'tp'), may hold values from -0.09375 to 0.09375
- gate_weight: bfloat16 [2, 4096, 32], replicated, may hold values from -0.09375 to 0.09375
- gate_bias: float32 [2, 32], replicated, may hold values from -1 to 3
- output_weight: bfloat16 [2, 3072, 4096], P(None, 'dp', 'tp'), may hold values from -0.109375 to 0.109375
- norm_gain: float32 [2, 4096], replicated, may hold values from 0.1 to 1.9
- matrix_state: float32 [2, 32, 192, 16, 192], P(None, 'dp', 'tp'), may hold values from -0.6 to 0.6
- normalizer_state: float32 [2, 32, 16, 192], P(None, 'dp'), may hold values from -0.6 to 0.6
- stabilizer_state: float32 [2, 32, 16], P(None, 'dp'), may hold values from -4 to 4
Outputs:
- out_stream: bfloat16 [32, 4096], P('dp', 'tp')
- new_matrix: float32 [2, 32, 192, 16, 192], P(None, 'dp', 'tp')
- new_normalizer: float32 [2, 32, 16, 192], P(None, 'dp')
- new_stabilizer: float32 [2, 32, 16], P(None, 'dp')
All inputs are finite; a program needn't handle non-finite values.
Results may differ from a plain program's by a relative error of at most 0.015.
Values may be sent and summed in bfloat16 or wider, within the bound.
A program may use at most 128 MiB of HBM per device.

v0:
```python
import jax
import jax.numpy as jnp
from jax import lax
from jax.sharding import PartitionSpec as P

residual_scale = 8.0**0.25
norm_eps = 1e-05


def normalize(values_in, gain):
    upcast = values_in.astype(jnp.float32)
    average = jnp.mean(upcast, axis=-1, keepdims=True)
    variance = jnp.mean(jnp.square(upcast - average), axis=-1, keepdims=True)
    return ((upcast - average) * lax.rsqrt(variance + norm_eps) * gain).astype(jnp.bfloat16)


def widen_rows(local_cols):
    return lax.all_gather(local_cols, "tp", axis=1, tiled=True)


def shards(
    stream,
    query_weight,
    key_weight,
    value_weight,
    outgate_weight,
    gate_weight,
    gate_bias,
    output_weight,
    norm_gain,
    matrix_state,
    normalizer_state,
    stabilizer_state,
):
    head_count = gate_bias.shape[1] // 2
    head_size = normalizer_state.shape[3]
    seq_local = stream.shape[0]
    feat_local = stream.shape[1]
    col_local = query_weight.shape[2]
    feat_offset = lax.axis_index("tp") * feat_local
    x_local = stream
    x_full = widen_rows(stream)
    new_mats, new_norms, new_stabs = ([], [], [])
    for block_no in range(gate_bias.shape[0]):
        weight_set = (
            query_weight[block_no],
            key_weight[block_no],
            value_weight[block_no],
            outgate_weight[block_no],
        )
        columns = x_full
        joined = jnp.concatenate(
            (
                lax.all_gather(weight_set[0], "dp", axis=0, tiled=True),
                lax.all_gather(weight_set[1], "dp", axis=0, tiled=True),
                lax.all_gather(weight_set[2], "dp", axis=0, tiled=True),
                lax.all_gather(weight_set[3], "dp", axis=0, tiled=True),
            ),
            axis=1,
        )
        packed = jnp.dot(columns, joined, preferred_element_type=jnp.float32)
        projected = packed.astype(jnp.bfloat16)
        query_part = projected[:, :col_local]
        key_part = projected[:, col_local : 2 * col_local]
        value_part = projected[:, 2 * col_local : 3 * col_local]
        outgate_part = projected[:, 3 * col_local :]
        query_full, key_full = (
            lax.all_gather(query_part, "tp", axis=1, tiled=True),
            lax.all_gather(key_part, "tp", axis=1, tiled=True),
        )
        gate_pre = (
            jnp.dot(x_full, gate_weight[block_no], preferred_element_type=jnp.float32)
            + gate_bias[block_no]
        )
        log_in = gate_pre[:, :head_count]
        log_forget = jax.nn.log_sigmoid(gate_pre[:, head_count:])
        old_stab = stabilizer_state[block_no]
        stab_new = jnp.maximum(log_forget + old_stab, log_in)
        retain = jnp.exp(log_forget + old_stab - stab_new)
        admit = jnp.exp(log_in - stab_new)
        queries = query_full.astype(jnp.float32).reshape(seq_local, head_count, head_size)
        keys = key_full.astype(jnp.float32).reshape(
            seq_local, head_count, head_size
        ) * head_size ** (-0.5)
        values = value_part.astype(jnp.float32).reshape(seq_local, -1, head_count)
        matrix = (
            retain[:, None, :, None] * matrix_state[block_no]
            + admit[:, None, :, None] * values[..., None] * keys[:, None, :, :]
        )
        norm_new = retain[..., None] * normalizer_state[block_no] + admit[..., None] * keys
        numerator = jnp.einsum("shd,sehd->seh", queries, matrix, precision=lax.Precision.HIGHEST)
        denominator = jnp.sum(queries * norm_new, axis=-1)
        divisor = jnp.maximum(jnp.abs(denominator), 1.0)
        readout = (numerator / divisor[:, None, :]).reshape(seq_local, col_local)
        hidden = (readout * jax.nn.sigmoid(outgate_part.astype(jnp.float32))).astype(jnp.bfloat16)
        hidden_full = lax.all_gather(hidden, "tp", axis=1, tiled=True)
        branch = jnp.dot(
            hidden_full,
            lax.all_gather(output_weight[block_no], "dp", axis=0, tiled=True),
            preferred_element_type=jnp.float32,
        )
        summed = (residual_scale * x_local.astype(jnp.float32) + branch).astype(jnp.bfloat16)
        x_full = normalize(widen_rows(summed), norm_gain[block_no])
        x_local = lax.dynamic_slice_in_dim(x_full, feat_offset, feat_local, 1)
        new_mats.append(matrix)
        new_norms.append(norm_new)
        new_stabs.append(stab_new)
    return (x_local, jnp.stack(new_mats), jnp.stack(new_norms), jnp.stack(new_stabs))


def solution(mesh):
    return jax.shard_map(
        shards,
        mesh=mesh,
        in_specs=(
            P("dp", "tp"),
            P(None, "dp", "tp"),
            P(None, "dp", "tp"),
            P(None, "dp", "tp"),
            P(None, "dp", "tp"),
            P(),
            P(),
            P(None, "dp", "tp"),
            P(),
            P(None, "dp", "tp", None, None),
            P(None, "dp", None, None),
            P(None, "dp", None),
        ),
        out_specs=(
            P("dp", "tp"),
            P(None, "dp", "tp", None, None),
            P(None, "dp", None, None),
            P(None, "dp", None),
        ),
        check_vma=False,
    )
```

profile of v0, /device:TPU:0, one launch (start us, length us, event | category | flops | bytes accessed | tf_op | source)
XLA Modules:
  0.0 442.6 jit_solution(219771178601658571)
XLA Ops:
  7.2 2.8 fusion.75
  10.1 1.3 fusion.76
  11.9 1.3 fusion.77
  13.3 1.3 fusion.78
  15.2 1.3 fusion.74
  19.9 32.4 %all_gather.57 = bf16[8,4096]{1,0:T(8,128)(2,1)S(1)} all-gather(bf16[8,512]{1,0:T(8,128)(2,1)S(1)} %copy-done.11), channel_id=1, replica_groups=mesh['tp'=8,'dp'=4] {'tp'}, dimensions={1}, use_global_device_ids=true | all-gather | bytes 73728 | tf_op jit(solution)/shard_map/all_gather | solution.py:18
  53.9 17.6 %all-gather.23.cloned.1.call-done = bf16[1,4096,384]{2,1,0:T(8,128)(2,1)} async-done(((bf16[1,1024,384]{2,1,0:T(8,128)(2,1)}), bf16[1,4096,384]{2,1,0:T(8,128)(2,1)}) %all-gather.23.cloned.1.call-update) | async-done | bytes 3145744 | tf_op jit(solution)/shard_map/all_gather | solution.py:55
  71.5 30.1 %all-gather.25.cloned.1.call-done = bf16[1,4096,384]{2,1,0:T(8,128)(2,1)} async-done(((bf16[1,1024,384]{2,1,0:T(8,128)(2,1)}), bf16[1,4096,384]{2,1,0:T(8,128)(2,1)}) %all-gather.25.cloned.1.call-update) | async-done | bytes 3145744 | tf_op jit(solution)/shard_map/all_gather | solution.py:56
  101.6 30.0 %all-gather.27.cloned.1.call-done = bf16[1,4096,384]{2,1,0:T(8,128)(2,1)} async-done(((bf16[1,1024,384]{2,1,0:T(8,128)(2,1)}), bf16[1,4096,384]{2,1,0:T(8,128)(2,1)}) %all-gather.27.cloned.1.call-update) | async-done | bytes 3145744 | tf_op jit(solution)/shard_map/all_gather | solution.py:57
  131.6 5.9 %fusion.32 = bf16[8,1536]{1,0:T(8,128)(2,1)S(1)} fusion(bf16[8,4096]{1,0:T(8,128)(2,1)S(1)} %all_gather.57, bf16[4096,384]{1,0:T(8,128)(2,1)} %bitcast.111, bf16[4096,384]{1,0:T(8,128)(2,1)} %bitcast.110, bf16[4096,384]{1,0:T(8,128)(2,1)} %bitcast.109, bf16[4096,384]{1,0:T(8,128)(2,1)} %bitcast.107), kind=kOutput, calls=%fused_computation.33 | convolution fusion | flops 151007232 | bytes 12673024 | tf_op jit(solution)/shard_map/dot_general | solution.py:61
  137.5 30.8 %all_gather.63 = bf16[8,3072]{1,0:T(8,128)(2,1)S(1)} all-gather(bf16[8,384]{1,0:T(8,128)(2,1)S(1)} %get-tuple-element.34), channel_id=1, replica_groups=mesh['tp'=8,'dp'=4] {'tp'}, dimensions={1}, use_global_device_ids=true | all-gather | bytes 55296 | tf_op jit(solution)/shard_map/all_gather | solution.py:68
  168.6 30.8 %all_gather.62 = bf16[8,3072]{1,0:T(8,128)(2,1)S(1)} all-gather(bf16[8,384]{1,0:T(8,128)(2,1)S(1)} %get-tuple-element.35), channel_id=1, replica_groups=mesh['tp'=8,'dp'=4] {'tp'}, dimensions={1}, use_global_device_ids=true | all-gather | bytes 55296 | tf_op jit(solution)/shard_map/all_gather | solution.py:69
  199.5 0.8 reshape.140
  200.6 2.9 fusion.21
  203.5 3.3 fusion.24
  207.0 30.8 %all_gather.64 = bf16[8,3072]{1,0:T(8,128)(2,1)S(1)} all-gather(bf16[8,384]{1,0:T(8,128)(2,1)S(1)} %multiply_convert_fusion.1), channel_id=1, replica_groups=mesh['tp'=8,'dp'=4] {'tp'}, dimensions={1}, use_global_device_ids=true | all-gather | bytes 55296 | tf_op jit(solution)/shard_map/all_gather | solution.py:96
  237.8 2.4 fusion.44
  240.2 30.5 %all_gather.66 = bf16[8,4096]{1,0:T(8,128)(2,1)S(1)} all-gather(bf16[8,512]{1,0:T(8,128)(2,1)S(1)} %fusion.44), channel_id=1, replica_groups=mesh['tp'=8,'dp'=4] {'tp'}, dimensions={1}, use_global_device_ids=true | all-gather | bytes 73728 | tf_op jit(solution)/shard_map/all_gather | solution.py:18
  271.4 11.0 %all-gather.37.cloned.1.call-done = bf16[1,4096,384]{2,1,0:T(8,128)(2,1)} async-done(((bf16[1,1024,384]{2,1,0:T(8,128)(2,1)}), bf16[1,4096,384]{2,1,0:T(8,128)(2,1)}) %all-gather.37.cloned.1.call-update) | async-done | bytes 3145744 | tf_op jit(solution)/shard_map/all_gather | solution.py:57
  282.3 5.9 %fusion.26 = bf16[8,1536]{1,0:T(8,128)(2,1)S(1)} fusion(bf16[8,4096]{1,0:T(8,128)(2,1)S(1)} %fusion.55, bf16[4096,384]{1,0:T(8,128)(2,1)} %bitcast.108, bf16[4096,384]{1,0:T(8,128)(2,1)} %bitcast.106, bf16[4096,384]{1,0:T(8,128)(2,1)} %bitcast.105, bf16[4096,384]{1,0:T(8,128)(2,1)} %bitcast.104), kind=kOutput, calls=%fused_computation.31 | convolution fusion | flops 151007232 | bytes 12673024 | tf_op jit(solution)/shard_map/dot_general | solution.py:61
  288.2 30.8 %all_gather.71 = bf16[8,3072]{1,0:T(8,128)(2,1)S(1)} all-gather(bf16[8,384]{1,0:T(8,128)(2,1)S(1)} %get-tuple-element.32), channel_id=1, replica_groups=mesh['tp'=8,'dp'=4] {'tp'}, dimensions={1}, use_global_device_ids=true | all-gather | bytes 55296 | tf_op jit(solution)/shard_map/all_gather | solution.py:69
  319.1 0.8 reshape.141
  320.0 31.0 %all_gather.72 = bf16[8,3072]{1,0:T(8,128)(2,1)S(1)} all-gather(bf16[8,384]{1,0:T(8,128)(2,1)S(1)} %get-tuple-element.31), channel_id=1, replica_groups=mesh['tp'=8,'dp'=4] {'tp'}, dimensions={1}, use_global_device_ids=true | all-gather | bytes 55296 | tf_op jit(solution)/shard_map/all_gather | solution.py:68
  352.4 2.4 fusion.18
  354.8 3.3 fusion.22
  358.4 32.6 %all_gather.73 = bf16[8,3072]{1,0:T(8,128)(2,1)} all-gather(bf16[8,384]{1,0:T(8,128)(2,1)S(1)} %multiply_convert_fusion), channel_id=1, replica_groups=mesh['tp'=8,'dp'=4] {'tp'}, dimensions={1}, use_global_device_ids=true | all-gather | bytes 55296 | tf_op jit(solution)/shard_map/all_gather | solution.py:96
  390.9 4.5 %multiply_add_fusion.1 = (f32[1,8,24,16,192]{4,3,2,1,0:T(8,128)S(1)}, f32[1,8,24,16,192]{4,3,2,1,0:T(8,128)}) fusion(f32[2,8,24,16,192]{4,3,2,1,0:T(8,128)} %param.21, f32[8,16,192]{2,1,0:T(8,128)S(1)} %get-tuple-element.25, f32[8,24,16]{2,1,0:T(8,128)S(1)} %broadcast_multiply_fusion.3, f32[8,16]{1,0:T(8,128)S(1)} %get-tuple-element.39, ...), kind=kLoop, calls=%fused_computation.30 | loop fusion | flops 3538944 | bytes 9659392 | tf_op jit(solution)/shard_map/add | solution.py:87
  395.5 2.6 fusion.41
  398.0 30.5 %all_gather.75 = bf16[8,4096]{1,0:T(8,128)(2,1)S(1)} all-gather(bf16[8,512]{1,0:T(8,128)(2,1)S(1)} %fusion.41), channel_id=1, replica_groups=mesh['tp'=8,'dp'=4] {'tp'}, dimensions={1}, use_global_device_ids=true | all-gather | bytes 73728 | tf_op jit(solution)/shard_map/all_gather | solution.py:18
  428.9 1.0 multiply_add_fusion.3
  430.0 0.7 pad_maximum_fusion.1
  430.7 3.7 pad_maximum_fusion
  (104 shorter events, 11.0 us)
Async XLA Ops:
  7.2 2.9 copy-start.1
  7.2 46.7 %all-gather.21.cloned.1.call-start = ((), (), s32[]{:S(2)}) async-start(), calls=%async_computation | async-start | bytes 3932160 | tf_op jit(solution)/shard_map/all_gather | solution.py:54
  10.0 1.9 copy-start.2
  10.0 61.5 %all-gather.23.cloned.1.call-start = ((), (), s32[]{:S(2)}) async-start(), calls=%async_computation.1 | async-start | bytes 3932160 | tf_op jit(solution)/shard_map/all_gather | solution.py:55
  11.4 1.9 copy-start.3
  11.4 90.2 %all-gather.25.cloned.1.call-start = ((), (), s32[]{:S(2)}) async-start(), calls=%async_computation.2 | async-start | bytes 3932160 | tf_op jit(solution)/shard_map/all_gather | solution.py:56
  13.2 1.9 copy-start.4
  13.3 118.3 %all-gather.27.cloned.1.call-start = ((), (), s32[]{:S(2)}) async-start(), calls=%async_computation.3 | async-start | bytes 3932160 | tf_op jit(solution)/shard_map/all_gather | solution.py:57
  14.7 223.1 %all-gather.29.cloned.1.call-start = ((), (), s32[]{:S(2)}) async-start(), calls=%async_computation.4 | async-start | bytes 3932160 | tf_op jit(solution)/shard_map/all_gather | solution.py:99
  16.4 3.5 copy-start.11
  16.4 35.8 %copy-start.17 = (f32[2,32]{1,0:T(2,128)S(1)}, f32[2,32]{1,0:T(2,128)}, u32[]{:S(2)}) copy-start(f32[2,32]{1,0:T(2,128)} %param.18) | copy-start | bytes 772
  16.4 35.8 %copy-start.12 = (f32[2,4096]{1,0:T(2,128)S(1)}, f32[2,4096]{1,0:T(2,128)}, u32[]{:S(2)}) copy-start(f32[2,4096]{1,0:T(2,128)} %param.20) | copy-start | bytes 98308
  16.5 35.9 %copy-start.9 = (bf16[2,4096,32]{1,2,0:T(8,128)(2,1)S(1)}, bf16[2,4096,32]{1,2,0:T(8,128)(2,1)}, u32[]{:S(2)}) copy-start(bf16[2,4096,32]{1,2,0:T(8,128)(2,1)} %param.17) | copy-start | bytes 1572868
  16.5 36.0 %copy-start.15 = (f32[2,8,16]{2,1,0:T(8,128)S(1)}, f32[2,8,16]{2,1,0:T(8,128)}, u32[]{:S(2)}) copy-start(f32[2,8,16]{2,1,0:T(8,128)} %param.23) | copy-start | bytes 3076
  16.5 254.8 %all-gather.31.cloned.1.call-start = ((), (), s32[]{:S(2)}) async-start(), calls=%async_computation.5 | async-start | bytes 3932160 | tf_op jit(solution)/shard_map/all_gather | solution.py:54
  17.1 254.3 %all-gather.33.cloned.1.call-start = ((), (), s32[]{:S(2)}) async-start(), calls=%async_computation.6 | async-start | bytes 3932160 | tf_op jit(solution)/shard_map/all_gather | solution.py:55
  17.8 253.5 %all-gather.35.cloned.1.call-start = ((), (), s32[]{:S(2)}) async-start(), calls=%async_computation.7 | async-start | bytes 3932160 | tf_op jit(solution)/shard_map/all_gather | solution.py:56
  18.6 263.8 %all-gather.37.cloned.1.call-start = ((), (), s32[]{:S(2)}) async-start(), calls=%async_computation.8 | async-start | bytes 3932160 | tf_op jit(solution)/shard_map/all_gather | solution.py:57
  19.3 376.1 %all-gather.39.cloned.1.call-start = ((), (), s32[]{:S(2)}) async-start(), calls=%async_computation.9 | async-start | bytes 3932160 | tf_op jit(solution)/shard_map/all_gather | solution.py:99
  131.6 68.9 %copy-start.5 = (f32[2,8,16,192]{3,2,1,0:T(8,128)S(1)}, f32[2,8,16,192]{3,2,1,0:T(8,128)}, u32[]{:S(2)}) copy-start(f32[2,8,16,192]{3,2,1,0:T(8,128)} %param.22) | copy-start | bytes 589828
  271.3 80.1 %copy-start.10 = (bf16[8,4096]{1,0:T(8,128)(2,1)}, bf16[8,4096]{1,0:T(8,128)(2,1)S(1)}, u32[]{:S(2)}) copy-start(bf16[8,4096]{1,0:T(8,128)(2,1)S(1)} %fusion.55) | copy-start | bytes 196612
  352.2 6.1 %copy-start.7 = (f32[8,24,16]{2,1,0:T(8,128)}, f32[8,24,16]{2,1,0:T(8,128)S(1)}, u32[]{:S(2)}) copy-start(f32[8,24,16]{2,1,0:T(8,128)S(1)} %broadcast_multiply_fusion.2) | copy-start | bytes 36868
  395.4 33.5 %copy-start.6 = (f32[2,8,16,192]{3,2,1,0:T(8,128)S(1)}, f32[2,8,16,192]{3,2,1,0:T(8,128)}, u32[]{:S(2)}) copy-start(f32[2,8,16,192]{3,2,1,0:T(8,128)} %param.22) | copy-start | bytes 589828
  395.4 33.5 %copy-start.8 = (f32[1,8,16,192]{3,2,1,0:T(8,128)S(1)}, f32[1,8,16,192]{3,2,1,0:T(8,128)}, u32[]{:S(2)}) copy-start(f32[1,8,16,192]{3,2,1,0:T(8,128)} %reshape.140) | copy-start | bytes 294916
  395.4 35.3 %copy-start = (f32[1,8,24,16,192]{4,3,2,1,0:T(8,128)S(1)}, f32[1,8,24,16,192]{4,3,2,1,0:T(8,128)}, u32[]{:S(2)}) copy-start(f32[1,8,24,16,192]{4,3,2,1,0:T(8,128)} %get-tuple-element.9) | copy-start | bytes 7077892
  430.7 3.7 copy-start.13
  430.7 3.7 copy-start.14
  430.7 4.4 copy-start.16
Sparse Core Ops, SparseCore 0:
  10.1 31.2 all-gather.20
  43.0 28.4 all-gather.22
  73.1 28.4 all-gather.24
  103.0 28.4 all-gather.26
  133.0 28.4 all-gather.28
  162.9 28.4 all-gather.30
  193.0 28.4 all-gather.32
  223.1 28.4 all-gather.34
  253.8 28.4 all-gather.36
  283.8 28.4 all-gather.38
where the time goes:
time: 443 us
  blocking collectives  280 us (63%)
  waiting for transfers between devices  92 us (21%)
  matrix products  23.7 us (5%)
  other arithmetic  19.2 us (4%)
  between operations  14.6 us (3%)
  local copies, waits for them, and re-layouts  12.6 us (3%)
    all_gather x3, blocking collectives, widen_rows(): return lax.all_gather(local_cols, 'tp', axis=1, tiled=True)  93.4 us
    all_gather x2, blocking collectives, shards(): hidden_full = lax.all_gather(hidden, 'tp', axis=1, tiled=True)  63.3 us
    all_gather x2, blocking collectives, shards(): lax.all_gather(query_part, 'tp', axis=1, tiled=True)  61.8 us
    all_gather x2, blocking collectives, shards(): lax.all_gather(key_part, 'tp', axis=1, tiled=True)  61.6 us
    all_gather x2, waiting for transfers between devices, shards(): lax.all_gather(weight_set[3], 'dp', axis=0, tiled=True)  40.9 us
    all_gather x2, waiting for transfers between devices, shards(): lax.all_gather(weight_set[2], 'dp', axis=0, tiled=True)  30.1 us
    all_gather x2, waiting for transfers between devices, shards(): lax.all_gather(weight_set[1], 'dp', axis=0, tiled=True)  17.7 us
    dot_general x2, matrix products, shards(): packed = jnp.dot(columns, joined, preferred_element_type=jnp.float32)  11.8 us
  transfers between devices with their start and end apart: 10, of which 4 were waited for; matrix products, arithmetic and copies ran while one was open for 10% of the time, Pallas kernels for 0%

commit v1 on v0

--- a/solution.py
+++ b/solution.py
@@ -93,7 +93,7 @@
         divisor = jnp.maximum(jnp.abs(denominator), 1.0)
         readout = (numerator / divisor[:, None, :]).reshape(seq_local, col_local)
         hidden = (readout * jax.nn.sigmoid(outgate_part.astype(jnp.float32))).astype(jnp.bfloat16)
-        hidden_full = lax.all_gather(hidden, "tp", axis=1, tiled=True)
+        hidden_full = jnp.concatenate(lax.all_gather(hidden, "tp"), axis=1)
         branch = jnp.dot(
             hidden_full,
             lax.all_gather(output_weight[block_no], "dp", axis=0, tiled=True),

time: 443 us -> 443 us (level)
  no operation moved by 1% of the time
where the time goes in v1:
time: 443 us
  blocking collectives  280 us (63%)
  waiting for transfers between devices  92 us (21%)
  matrix products  23.7 us (5%)
  other arithmetic  19.2 us (4%)
  between operations  14.6 us (3%)
  local copies, waits for them, and re-layouts  12.6 us (3%)
    all_gather x3, blocking collectives, widen_rows(): return lax.all_gather(local_cols, 'tp', axis=1, tiled=True)  93.4 us
    all_gather x2, blocking collectives, shards(): hidden_full = jnp.concatenate(lax.all_gather(hidden, 'tp'), axis=1)  63.3 us
    all_gather x2, blocking collectives, shards(): lax.all_gather(query_part, 'tp', axis=1, tiled=True)  61.8 us
    all_gather x2, blocking collectives, shards(): lax.all_gather(key_part, 'tp', axis=1, tiled=True)  61.6 us
    all_gather x2, waiting for transfers between devices, shards(): lax.all_gather(weight_set[3], 'dp', axis=0, tiled=True)  40.9 us
    all_gather x2, waiting for transfers between devices, shards(): lax.all_gather(weight_set[2], 'dp', axis=0, tiled=True)  30.1 us
    all_gather x2, waiting for transfers between devices, shards(): lax.all_gather(weight_set[1], 'dp', axis=0, tiled=True)  17.7 us
    dot_general x2, matrix products, shards(): packed = jnp.dot(columns, joined, preferred_element_type=jnp.float32)  11.8 us
  transfers between devices with their start and end apart: 10, of which 4 were waited for; matrix products, arithmetic and copies ran while one was open for 10% of the time, Pallas kernels for 0%

profile of v1, /device:TPU:0, one launch (start us, length us, event | category | flops | bytes accessed | tf_op | source)
XLA Modules:
  0.0 442.6 jit_solution(15918312324915583625)
XLA Ops:
  7.2 2.8 fusion.75
  10.1 1.3 fusion.76
  11.9 1.3 fusion.77
  13.3 1.3 fusion.78
  15.2 1.3 fusion.74
  19.9 32.4 %all_gather.63 = bf16[8,4096]{1,0:T(8,128)(2,1)S(1)} all-gather(bf16[8,512]{1,0:T(8,128)(2,1)S(1)} %copy-done.11), channel_id=1, replica_groups=mesh['tp'=8,'dp'=4] {'tp'}, dimensions={1}, use_global_device_ids=true | all-gather | bytes 73728 | tf_op jit(solution)/shard_map/all_gather | solution.py:18
  53.9 17.6 %all-gather.25.cloned.1.call-done = bf16[1,4096,384]{2,1,0:T(8,128)(2,1)} async-done(((bf16[1,1024,384]{2,1,0:T(8,128)(2,1)}), bf16[1,4096,384]{2,1,0:T(8,128)(2,1)}) %all-gather.25.cloned.1.call-update) | async-done | bytes 3145744 | tf_op jit(solution)/shard_map/all_gather | solution.py:55
  71.5 30.1 %all-gather.27.cloned.1.call-done = bf16[1,4096,384]{2,1,0:T(8,128)(2,1)} async-done(((bf16[1,1024,384]{2,1,0:T(8,128)(2,1)}), bf16[1,4096,384]{2,1,0:T(8,128)(2,1)}) %all-gather.27.cloned.1.call-update) | async-done | bytes 3145744 | tf_op jit(solution)/shard_map/all_gather | solution.py:56
  101.6 30.0 %all-gather.29.cloned.1.call-done = bf16[1,4096,384]{2,1,0:T(8,128)(2,1)} async-done(((bf16[1,1024,384]{2,1,0:T(8,128)(2,1)}), bf16[1,4096,384]{2,1,0:T(8,128)(2,1)}) %all-gather.29.cloned.1.call-update) | async-done | bytes 3145744 | tf_op jit(solution)/shard_map/all_gather | solution.py:57
  131.6 5.9 %fusion.32 = bf16[8,1536]{1,0:T(8,128)(2,1)S(1)} fusion(bf16[8,4096]{1,0:T(8,128)(2,1)S(1)} %all_gather.63, bf16[4096,384]{1,0:T(8,128)(2,1)} %bitcast.123, bf16[4096,384]{1,0:T(8,128)(2,1)} %bitcast.122, bf16[4096,384]{1,0:T(8,128)(2,1)} %bitcast.121, bf16[4096,384]{1,0:T(8,128)(2,1)} %bitcast.119), kind=kOutput, calls=%fused_computation.33 | convolution fusion | flops 151007232 | bytes 12673024 | tf_op jit(solution)/shard_map/dot_general | solution.py:61
  137.5 30.8 %all_gather.69 = bf16[8,3072]{1,0:T(8,128)(2,1)S(1)} all-gather(bf16[8,384]{1,0:T(8,128)(2,1)S(1)} %get-tuple-element.34), channel_id=1, replica_groups=mesh['tp'=8,'dp'=4] {'tp'}, dimensions={1}, use_global_device_ids=true | all-gather | bytes 55296 | tf_op jit(solution)/shard_map/all_gather | solution.py:68
  168.6 30.8 %all_gather.68 = bf16[8,3072]{1,0:T(8,128)(2,1)S(1)} all-gather(bf16[8,384]{1,0:T(8,128)(2,1)S(1)} %get-tuple-element.35), channel_id=1, replica_groups=mesh['tp'=8,'dp'=4] {'tp'}, dimensions={1}, use_global_device_ids=true | all-gather | bytes 55296 | tf_op jit(solution)/shard_map/all_gather | solution.py:69
  199.5 0.8 reshape.156
  200.6 2.9 fusion.21
  203.5 3.3 fusion.24
  207.0 30.8 %all-gather.4 = bf16[64,384]{1,0:T(8,128)(2,1)S(1)} all-gather(bf16[8,384]{1,0:T(8,128)(2,1)S(1)} %multiply_convert_fusion.1), channel_id=6, replica_groups=mesh['tp'=8,'dp'=4] {'tp'}, dimensions={0}, use_global_device_ids=true | all-gather | bytes 55296 | tf_op jit(solution)/shard_map/all_gather | solution.py:96
  237.8 2.4 fusion.44
  240.2 30.5 %all_gather.73 = bf16[8,4096]{1,0:T(8,128)(2,1)S(1)} all-gather(bf16[8,512]{1,0:T(8,128)(2,1)S(1)} %fusion.44), channel_id=1, replica_groups=mesh['tp'=8,'dp'=4] {'tp'}, dimensions={1}, use_global_device_ids=true | all-gather | bytes 73728 | tf_op jit(solution)/shard_map/all_gather | solution.py:18
  271.4 11.0 %all-gather.39.cloned.1.call-done = bf16[1,4096,384]{2,1,0:T(8,128)(2,1)} async-done(((bf16[1,1024,384]{2,1,0:T(8,128)(2,1)}), bf16[1,4096,384]{2,1,0:T(8,128)(2,1)}) %all-gather.39.cloned.1.call-update) | async-done | bytes 3145744 | tf_op jit(solution)/shard_map/all_gather | solution.py:57
  282.3 5.9 %fusion.26 = bf16[8,1536]{1,0:T(8,128)(2,1)S(1)} fusion(bf16[8,4096]{1,0:T(8,128)(2,1)S(1)} %fusion.55, bf16[4096,384]{1,0:T(8,128)(2,1)} %bitcast.120, bf16[4096,384]{1,0:T(8,128)(2,1)} %bitcast.118, bf16[4096,384]{1,0:T(8,128)(2,1)} %bitcast.117, bf16[4096,384]{1,0:T(8,128)(2,1)} %bitcast.116), kind=kOutput, calls=%fused_computation.31 | convolution fusion | flops 151007232 | bytes 12673024 | tf_op jit(solution)/shard_map/dot_general | solution.py:61
  288.2 30.8 %all_gather.78 = bf16[8,3072]{1,0:T(8,128)(2,1)S(1)} all-gather(bf16[8,384]{1,0:T(8,128)(2,1)S(1)} %get-tuple-element.32), channel_id=1, replica_groups=mesh['tp'=8,'dp'=4] {'tp'}, dimensions={1}, use_global_device_ids=true | all-gather | bytes 55296 | tf_op jit(solution)/shard_map/all_gather | solution.py:69
  319.1 0.8 reshape.157
  320.0 31.0 %all_gather.79 = bf16[8,3072]{1,0:T(8,128)(2,1)S(1)} all-gather(bf16[8,384]{1,0:T(8,128)(2,1)S(1)} %get-tuple-element.31), channel_id=1, replica_groups=mesh['tp'=8,'dp'=4] {'tp'}, dimensions={1}, use_global_device_ids=true | all-gather | bytes 55296 | tf_op jit(solution)/shard_map/all_gather | solution.py:68
  352.4 2.4 fusion.18
  354.8 3.3 fusion.22
  358.4 32.6 %all-gather.10 = bf16[64,384]{1,0:T(8,128)(2,1)} all-gather(bf16[8,384]{1,0:T(8,128)(2,1)S(1)} %multiply_convert_fusion), channel_id=12, replica_groups=mesh['tp'=8,'dp'=4] {'tp'}, dimensions={0}, use_global_device_ids=true | all-gather | bytes 55296 | tf_op jit(solution)/shard_map/all_gather | solution.py:96
  390.9 4.5 %multiply_add_fusion.1 = (f32[1,8,24,16,192]{4,3,2,1,0:T(8,128)S(1)}, f32[1,8,24,16,192]{4,3,2,1,0:T(8,128)}) fusion(f32[2,8,24,16,192]{4,3,2,1,0:T(8,128)} %param.21, f32[8,16,192]{2,1,0:T(8,128)S(1)} %get-tuple-element.25, f32[8,24,16]{2,1,0:T(8,128)S(1)} %broadcast_multiply_fusion.3, f32[8,16]{1,0:T(8,128)S(1)} %get-tuple-element.39, ...), kind=kLoop, calls=%fused_computation.30 | loop fusion | flops 3538944 | bytes 9659392 | tf_op jit(solution)/shard_map/add | solution.py:87
  395.5 2.6 fusion.41
  398.0 30.5 %all_gather.83 = bf16[8,4096]{1,0:T(8,128)(2,1)S(1)} all-gather(bf16[8,512]{1,0:T(8,128)(2,1)S(1)} %fusion.41), channel_id=1, replica_groups=mesh['tp'=8,'dp'=4] {'tp'}, dimensions={1}, use_global_device_ids=true | all-gather | bytes 73728 | tf_op jit(solution)/shard_map/all_gather | solution.py:18
  428.9 1.0 multiply_add_fusion.3
  430.0 0.7 pad_maximum_fusion.1
  430.7 3.7 pad_maximum_fusion
  (104 shorter events, 11.0 us)
Async XLA Ops:
  7.2 2.9 copy-start.1
  7.2 46.7 %all-gather.23.cloned.1.call-start = ((), (), s32[]{:S(2)}) async-start(), calls=%async_computation | async-start | bytes 3932160 | tf_op jit(solution)/shard_map/all_gather | solution.py:54
  10.0 1.9 copy-start.2
  10.0 61.5 %all-gather.25.cloned.1.call-start = ((), (), s32[]{:S(2)}) async-start(), calls=%async_computation.1 | async-start | bytes 3932160 | tf_op jit(solution)/shard_map/all_gather | solution.py:55
  11.4 1.9 copy-start.3
  11.4 90.2 %all-gather.27.cloned.1.call-start = ((), (), s32[]{:S(2)}) async-start(), calls=%async_computation.2 | async-start | bytes 3932160 | tf_op jit(solution)/shard_map/all_gather | solution.py:56
  13.2 1.9 copy-start.4
  13.3 118.3 %all-gather.29.cloned.1.call-start = ((), (), s32[]{:S(2)}) async-start(), calls=%async_computation.3 | async-start | bytes 3932160 | tf_op jit(solution)/shard_map/all_gather | solution.py:57
  14.7 223.1 %all-gather.31.cloned.1.call-start = ((), (), s32[]{:S(2)}) async-start(), calls=%async_computation.4 | async-start | bytes 3932160 | tf_op jit(solution)/shard_map/all_gather | solution.py:99
  16.4 3.5 copy-start.11
  16.4 35.8 %copy-start.17 = (f32[2,32]{1,0:T(2,128)S(1)}, f32[2,32]{1,0:T(2,128)}, u32[]{:S(2)}) copy-start(f32[2,32]{1,0:T(2,128)} %param.18) | copy-start | bytes 772
  16.4 35.8 %copy-start.12 = (f32[2,4096]{1,0:T(2,128)S(1)}, f32[2,4096]{1,0:T(2,128)}, u32[]{:S(2)}) copy-start(f32[2,4096]{1,0:T(2,128)} %param.20) | copy-start | bytes 98308
  16.5 35.9 %copy-start.9 = (bf16[2,4096,32]{1,2,0:T(8,128)(2,1)S(1)}, bf16[2,4096,32]{1,2,0:T(8,128)(2,1)}, u32[]{:S(2)}) copy-start(bf16[2,4096,32]{1,2,0:T(8,128)(2,1)} %param.17) | copy-start | bytes 1572868
  16.5 36.0 %copy-start.15 = (f32[2,8,16]{2,1,0:T(8,128)S(1)}, f32[2,8,16]{2,1,0:T(8,128)}, u32[]{:S(2)}) copy-start(f32[2,8,16]{2,1,0:T(8,128)} %param.23) | copy-start | bytes 3076
  16.5 254.8 %all-gather.33.cloned.1.call-start = ((), (), s32[]{:S(2)}) async-start(), calls=%async_computation.5 | async-start | bytes 3932160 | tf_op jit(solution)/shard_map/all_gather | solution.py:54
  17.1 254.3 %all-gather.35.cloned.1.call-start = ((), (), s32[]{:S(2)}) async-start(), calls=%async_computation.6 | async-start | bytes 3932160 | tf_op jit(solution)/shard_map/all_gather | solution.py:55
  17.8 253.5 %all-gather.37.cloned.1.call-start = ((), (), s32[]{:S(2)}) async-start(), calls=%async_computation.7 | async-start | bytes 3932160 | tf_op jit(solution)/shard_map/all_gather | solution.py:56
  18.6 263.8 %all-gather.39.cloned.1.call-start = ((), (), s32[]{:S(2)}) async-start(), calls=%async_computation.8 | async-start | bytes 3932160 | tf_op jit(solution)/shard_map/all_gather | solution.py:57
  19.3 376.1 %all-gather.41.cloned.1.call-start = ((), (), s32[]{:S(2)}) async-start(), calls=%async_computation.9 | async-start | bytes 3932160 | tf_op jit(solution)/shard_map/all_gather | solution.py:99
  131.6 68.9 %copy-start.5 = (f32[2,8,16,192]{3,2,1,0:T(8,128)S(1)}, f32[2,8,16,192]{3,2,1,0:T(8,128)}, u32[]{:S(2)}) copy-start(f32[2,8,16,192]{3,2,1,0:T(8,128)} %param.22) | copy-start | bytes 589828
  271.3 80.1 %copy-start.10 = (bf16[8,4096]{1,0:T(8,128)(2,1)}, bf16[8,4096]{1,0:T(8,128)(2,1)S(1)}, u32[]{:S(2)}) copy-start(bf16[8,4096]{1,0:T(8,128)(2,1)S(1)} %fusion.55) | copy-start | bytes 196612
  352.2 6.1 %copy-start.7 = (f32[8,24,16]{2,1,0:T(8,128)}, f32[8,24,16]{2,1,0:T(8,128)S(1)}, u32[]{:S(2)}) copy-start(f32[8,24,16]{2,1,0:T(8,128)S(1)} %broadcast_multiply_fusion.2) | copy-start | bytes 36868
  395.4 33.5 %copy-start.6 = (f32[2,8,16,192]{3,2,1,0:T(8,128)S(1)}, f32[2,8,16,192]{3,2,1,0:T(8,128)}, u32[]{:S(2)}) copy-start(f32[2,8,16,192]{3,2,1,0:T(8,128)} %param.22) | copy-start | bytes 589828
  395.4 33.5 %copy-start.8 = (f32[1,8,16,192]{3,2,1,0:T(8,128)S(1)}, f32[1,8,16,192]{3,2,1,0:T(8,128)}, u32[]{:S(2)}) copy-start(f32[1,8,16,192]{3,2,1,0:T(8,128)} %reshape.156) | copy-start | bytes 294916
  395.4 35.3 %copy-start = (f32[1,8,24,16,192]{4,3,2,1,0:T(8,128)S(1)}, f32[1,8,24,16,192]{4,3,2,1,0:T(8,128)}, u32[]{:S(2)}) copy-start(f32[1,8,24,16,192]{4,3,2,1,0:T(8,128)} %get-tuple-element.9) | copy-start | bytes 7077892
  430.7 3.7 copy-start.13
  430.7 3.7 copy-start.14
  430.7 4.4 copy-start.16
Sparse Core Ops, SparseCore 0:
  10.1 31.2 all-gather.22
  43.0 28.4 all-gather.24
  73.1 28.4 all-gather.26
  103.0 28.4 all-gather.28
  133.0 28.4 all-gather.30
  162.9 28.4 all-gather.32
  193.0 28.4 all-gather.34
  223.1 28.4 all-gather.36
  253.8 28.4 all-gather.38
  283.8 28.4 all-gather.40
